TPU v7x, 32 devices: a whole 2x2x4 slice. The times are simulated.
32 devices in a mesh: ep: 8 (over z, x), tp: 4 (over y, core).
Axes of the slice: x: 2, y: 2, z: 4, core: 2. Of those that a mesh axis runs over, the one named last changes fastest.
Arguments:
- q_in: bfloat16 [4096, 1024], P('ep', 'tp'), may hold values from -6 to 6
- k_in: bfloat16 [4096, 256], P('ep'), may hold values from -6 to 6
- v_in: bfloat16 [4096, 256], P('ep'), may hold values from -6 to 6
- q_gain: float32 [64], replicated, may hold values from 0.1 to 1.9
- k_gain: float32 [64], replicated, may hold values from 0.1 to 1.9
- w_out: bfloat16 [1024, 2048], P('tp'), may hold values from -0.1875 to 0.1875
- post_gain: float32 [2048], replicated, may hold values from 0.1 to 1.9
- moe_in: bfloat16 [1024, 2048], P('ep'), may hold values from -6 to 6
- routes: int32 [1024, 2], P('ep'), may hold values from 0 to 7, all different within a row; in each aligned block of 128 rows (0 to 127, 128 to 255, ...) at most 48 rows name the same one
- route_logits: float32 [1024, 2], P('ep'), may hold values from -6 to 6
- pre_gain: float32 [2048], replicated, may hold values from 0.1 to 1.9
- w_gate: bfloat16 [8, 2048, 4096], P('ep', None, 'tp'), may hold values from -0.125 to 0.125
- w_up: bfloat16 [8, 2048, 4096], P('ep', None, 'tp'), may hold values from -0.125 to 0.125
- w_down: bfloat16 [8, 4096, 2048], P('ep', 'tp'), may hold values from -0.125 to 0.125
Outputs:
- attn_out: bfloat16 [4096, 2048], P(('ep', 'tp'))
- moe_out: bfloat16 [1024, 2048], P('ep', 'tp')
Inputs may be any that keep to these rules, and one draw needn't show every extreme that they name: `routes`: each row names 2 different experts. Among the rows of one index of ep no expert is named by more than 48 rows, a bound that some block reaches of them.
All inputs are finite; a program needn't handle non-finite values.
Results may differ from a plain program's by a relative error of at most 0.018.
Values may be sent and summed in bfloat16 or wider, within the bound.
A program may use at most 64 MiB of HBM per device.

v0:
```python
import jax
import jax.numpy as jnp
from jax import lax
from jax.sharding import PartitionSpec as P

GRID_W = 128


EPSILON = 1e-06
ROPE_BASE = 10000.0


def head_norm(values, gain):
    return values * lax.rsqrt(jnp.mean(values * values, axis=-1, keepdims=True) + EPSILON) * gain


def rotate_half(values, angles):
    quarter = angles.shape[-1]
    first_part = values[..., :quarter]
    second_part = values[..., quarter:]
    cosine = jnp.cos(angles)[:, None, :]
    sine_part = jnp.sin(angles)[:, None, :]
    return jnp.concatenate(
        [
            first_part * cosine - second_part * sine_part,
            second_part * cosine + first_part * sine_part,
        ],
        axis=-1,
    )


def grid_rotary(values, offset):
    row_count = values.shape[0]
    head_width = values.shape[-1]
    quarter = head_width // 4
    half_width = head_width // 2
    position = offset + jnp.arange(row_count, dtype=jnp.int32)
    grid_row = (position // GRID_W).astype(jnp.float32)
    grid_col = (position % GRID_W).astype(jnp.float32)
    inverse = ROPE_BASE ** (-jnp.arange(quarter, dtype=jnp.float32) / quarter)
    return jnp.concatenate(
        [
            rotate_half(values[..., :half_width], grid_row[:, None] * inverse[None, :]),
            rotate_half(values[..., half_width:], grid_col[:, None] * inverse[None, :]),
        ],
        axis=-1,
    )


def slot_table(route_rows, expert_count, capacity):
    token_count, top_count = route_rows.shape
    flat_routes = route_rows.reshape(-1)
    one_hot = (flat_routes[:, None] == jnp.arange(expert_count, dtype=jnp.int32)[None, :]).astype(
        jnp.int32
    )
    ranked = jnp.sum((jnp.cumsum(one_hot, axis=0) - 1) * one_hot, axis=1)
    placed = flat_routes * capacity + ranked
    slot_owner = jnp.full((expert_count * capacity,), token_count * top_count, dtype=jnp.int32)
    slot_owner = slot_owner.at[placed].set(jnp.arange(token_count * top_count, dtype=jnp.int32))
    return (slot_owner, placed)


def mixer_half(q_in, k_in, v_in, q_gain, k_gain, w_out, post_gain):
    head_size = q_gain.shape[0]
    row_count = q_in.shape[0]
    local_heads = q_in.shape[1] // head_size
    kv_count = k_in.shape[1] // head_size
    tp_count = lax.axis_size("tp")
    repeat = local_heads * tp_count // kv_count
    offset = lax.axis_index("ep") * row_count
    queries = head_norm(q_in.astype(jnp.float32).reshape(row_count, local_heads, head_size), q_gain)
    queries = grid_rotary(queries, offset).astype(jnp.bfloat16)
    query_rows = jnp.transpose(queries, (1, 0, 2)).reshape(local_heads * row_count, head_size)
    kv_index = lax.axis_index("tp") * local_heads // repeat
    own_keys = lax.dynamic_slice_in_dim(k_in, kv_index * head_size, head_size, 1)
    own_values = lax.dynamic_slice_in_dim(v_in, kv_index * head_size, head_size, 1)
    own_keys = head_norm(own_keys.astype(jnp.float32)[:, None, :], k_gain)
    own_keys = grid_rotary(own_keys, offset)[:, 0, :].astype(jnp.bfloat16)
    paired = jnp.concatenate([own_keys, own_values], axis=1)
    scale_factor = head_size ** (-0.5)

    def attend_block(running, key_block):
        block_keys = key_block[:, :head_size]
        block_values = key_block[:, head_size:]
        scores = (
            jnp.einsum("qd,kd->qk", query_rows, block_keys, preferred_element_type=jnp.float32)
            * scale_factor
        )
        weights = jnp.exp(scores)
        numer = running[0] + jnp.dot(
            weights.astype(jnp.bfloat16), block_values, preferred_element_type=jnp.float32
        )
        return (numer, running[1] + jnp.sum(weights, axis=1))

    zero_init = (
        jnp.zeros((local_heads * row_count, head_size), jnp.float32),
        jnp.zeros((local_heads * row_count,), jnp.float32),
    )
    running = zero_init
    gathered_piece = lax.all_gather(paired, "ep", axis=0, tiled=True)
    piece_rows = gathered_piece.shape[0]
    blocks = gathered_piece.reshape(piece_rows // 512, 512, gathered_piece.shape[1])

    def scan_block(partial_value, key_block):
        return (attend_block(partial_value, key_block), None)

    running, unused = lax.scan(scan_block, running, blocks)
    numer, denom = running
    head_out = (numer / denom[:, None]).astype(jnp.bfloat16)
    head_out = jnp.transpose(head_out.reshape(local_heads, row_count, head_size), (1, 0, 2))
    head_out = head_out.reshape(row_count, local_heads * head_size)
    mixed = lax.psum_scatter(
        jnp.dot(head_out, w_out, preferred_element_type=jnp.float32).astype(jnp.bfloat16),
        "tp",
        scatter_dimension=0,
        tiled=True,
    ).astype(jnp.float32)
    return head_norm(mixed, post_gain).astype(jnp.bfloat16)


def experts_half(moe_in, routes, route_logits, pre_gain, w_gate, w_up, w_down):
    token_count, top_count = routes.shape
    model_width = moe_in.shape[1]
    expert_count = lax.axis_size("ep")
    capacity = max(2, 3 * top_count * token_count // (2 * expert_count))
    tp_count = lax.axis_size("tp")
    slice_width = model_width // tp_count
    normed = head_norm(moe_in.astype(jnp.float32), pre_gain).astype(jnp.bfloat16)
    slot_owner, placed = slot_table(routes, expert_count, capacity)
    padded = jnp.concatenate([normed, jnp.zeros((1, model_width), jnp.bfloat16)], axis=0)
    outgoing = padded[slot_owner // top_count].reshape(expert_count, capacity, model_width)
    arrived = lax.all_to_all(outgoing, "ep", split_axis=0, concat_axis=0, tiled=True)
    arrived = arrived.reshape(expert_count * capacity, model_width)
    gate_pre = jnp.dot(arrived, w_gate[0], preferred_element_type=jnp.float32)
    up_pre = jnp.dot(arrived, w_up[0], preferred_element_type=jnp.float32)
    hidden = (jax.nn.silu(gate_pre) * up_pre).astype(jnp.bfloat16)
    partial_out = jnp.dot(hidden, w_down[0], preferred_element_type=jnp.float32)
    partial_out = partial_out.reshape(expert_count, capacity, model_width)
    summed = lax.psum_scatter(
        partial_out.astype(jnp.bfloat16), "tp", scatter_dimension=2, tiled=True
    )
    returned = lax.all_to_all(summed, "ep", split_axis=0, concat_axis=0, tiled=True)
    returned = returned.reshape(expert_count * capacity, slice_width)
    copies = returned[placed].reshape(token_count, top_count, slice_width).astype(jnp.float32)
    route_weight = jax.nn.softmax(route_logits, axis=-1)
    return jnp.sum(route_weight[..., None] * copies, axis=1).astype(jnp.bfloat16)


def per_device(
    q_in,
    k_in,
    v_in,
    q_gain,
    k_gain,
    w_out,
    post_gain,
    moe_in,
    routes,
    route_logits,
    pre_gain,
    w_gate,
    w_up,
    w_down,
):
    attn_out = mixer_half(q_in, k_in, v_in, q_gain, k_gain, w_out, post_gain)
    moe_out = experts_half(moe_in, routes, route_logits, pre_gain, w_gate, w_up, w_down)
    return (attn_out, moe_out)


def solution(mesh):
    return jax.shard_map(
        per_device,
        mesh=mesh,
        in_specs=(
            P("ep", "tp"),
            P("ep", None),
            P("ep", None),
            P(),
            P(),
            P("tp", None),
            P(),
            P("ep", None),
            P("ep", None),
            P("ep", None),
            P(),
            P("ep", None, "tp"),
            P("ep", None, "tp"),
            P("ep", "tp", None),
        ),
        out_specs=(P(("ep", "tp"), None), P("ep", "tp")),
        check_vma=False,
    )
```

profile of v0, /device:TPU:9, one launch (start us, length us, event | category | flops | bytes accessed | tf_op | source)
XLA Modules:
  0.0 184.2 jit_solution(11214696343545034479)
XLA Ops:
  15.0 3.1 %gather_fusion = bf16[384,2048]{1,0:T(8,128)(2,1)} fusion(bf16[129,2048]{1,0:T(8,128)(2,1)S(1)} %concatenate.17, s32[1024]{0:T(1024)S(1)} %pad_clamp_fusion.1), kind=kCustom, calls=%fused_computation | custom fusion | bytes 3147264 | tf_op jit(solution)/shard_map/gather | solution.py:131
  18.2 5.8 %all-to-all-start = ((bf16[8,48,2048]{2,1,0:T(8,128)(2,1)}), bf16[8,48,2048]{2,1,0:T(8,128)(2,1)}, u32[]{:S(2)}, u32[]{:S(2)}) async-start(bf16[8,48,2048]{2,1,0:T(8,128)(2,1)} %bitcast.13), calls=%async_computation.1 | async-start | bytes 3145728 | tf_op jit(solution)/shard_map/all_to_all | solution.py:132
  26.7 47.9 %all-gather.2.cloned.1.call-done = bf16[4096,128]{0,1:T(8,128)(2,1)} async-done(((bf16[512,128]{0,1:T(8,128)(2,1)}), bf16[4096,128]{0,1:T(8,128)(2,1)}) %all-gather.2.cloned.1.call-update) | async-done | bytes 1048592 | tf_op jit(solution)/shard_map/all_gather | solution.py:100
  76.3 4.6 %fusion.12 = f32[384,1024]{1,0:T(8,128)S(1)} fusion(bf16[384,2048]{1,0:T(8,128)(2,1)} %bitcast.14, bf16[1,2048,1024]{2,1,0:T(8,128)(2,1)} %param.27), kind=kOutput, calls=%fused_computation.18 | convolution fusion | flops 1610612736 | bytes 7340032 | tf_op jit(solution)/shard_map/dot_general | solution.py:134
  80.9 3.5 %multiply_convert_fusion = bf16[384,1024]{1,0:T(8,128)(2,1)S(1)} fusion(f32[384,1024]{1,0:T(8,128)S(1)} %fusion.12, bf16[384,2048]{1,0:T(8,128)(2,1)} %bitcast.14, bf16[1,2048,1024]{2,1,0:T(8,128)(2,1)S(1)} %copy-done.8), kind=kOutput, calls=%fused_computation.22 | convolution fusion | flops 1612972032 | bytes 8126464 | tf_op jit(solution)/shard_map/dot_general | solution.py:135
  84.4 3.0 %fusion.14 = bf16[8,48,2048]{2,1,0:T(8,128)(2,1)} fusion(bf16[8,48,1024]{2,1,0:T(8,128)(2,1)S(1)} %bitcast.62, bf16[1,1024,2048]{2,1,0:T(8,128)(2,1)S(1)} %copy-done.9), kind=kOutput, calls=%fused_computation.21 | convolution fusion | flops 1611399168 | bytes 6553600 | tf_op jit(solution)/shard_map/dot_general | solution.py:137
  87.5 46.5 %while.13 = (s32[]{:T(128)}, f32[2048,64]{0,1:T(8,128)S(1)}, f32[2048]{0:T(1024)S(1)}, bf16[8,512,128]{2,1,0:T(8,128)(2,1)S(1)}, bf16[2048,64]{1,0:T(8,128)(2,1)S(1)}, /*index=5*/s32[]{:T(128)}, s32[]{:T(128)}) while((s32[]{:T(128)}, f32[2048,64]{0,1:T(8,128)S(1)}, f32[2048]{0:T(1024)S(1)}, bf16[8,512,128]{2,1,0:T(8,128)(2,1)S(1)}, ...), condition=%wide.region_4.5_spmd.clone, body=%wide.region_2.4_spmd.clone.sunk | while | flops 272893952 | bytes 10256476 | solution.py:107
  87.6 2.7 %fusion.72 = (f32[2048]{0:T(1024)S(1)}, f32[512,2048]{1,0:T(8,128)}) fusion(bf16[2048,64]{1,0:T(8,128)(2,1)S(1)} %get-tuple-element.147, bf16[512,128]{1,0:T(8,128)(2,1)S(1)} %dynamic-slice_bitcast_fusion.2), kind=kOutput, calls=%fused_computation.4.clone.1 | convolution fusion | flops 136312832 | bytes 4595712 | tf_op jit(solution)/shard_map/while/body/eval_jaxpr/qd,kd->qk/dot_general | solution.py:86
  90.2 3.1 %convolution_add_fusion.2 = f32[2048,64]{0,1:T(8,128)S(1)} fusion(f32[512,2048]{1,0:T(8,128)} %get-tuple-element.127, f32[2048,64]{0,1:T(8,128)S(1)} %get-tuple-element.137, pred[]{:T(512)S(6)} %compare.19, bf16[512,128]{1,0:T(8,128)(2,1)S(1)} %dynamic-slice_bitcast_fusion.2), kind=kOutput, calls=%fused_computation.6.clone.1 | convolution fusion | flops 136577024 | bytes 5373953 | tf_op jit(solution)/shard_map/while/body/eval_jaxpr/dot_general | solution.py:90
  93.3 2.7 %fusion.72 = (f32[2048]{0:T(1024)S(1)}, f32[512,2048]{1,0:T(8,128)}) fusion(bf16[2048,64]{1,0:T(8,128)(2,1)S(1)} %get-tuple-element.147, bf16[512,128]{1,0:T(8,128)(2,1)S(1)} %dynamic-slice_bitcast_fusion.2), kind=kOutput, calls=%fused_computation.4.clone.1 | convolution fusion | flops 136312832 | bytes 4595712 | tf_op jit(solution)/shard_map/while/body/eval_jaxpr/qd,kd->qk/dot_general | solution.py:86
  96.0 3.2 %convolution_add_fusion.2 = f32[2048,64]{0,1:T(8,128)S(1)} fusion(f32[512,2048]{1,0:T(8,128)} %get-tuple-element.127, f32[2048,64]{0,1:T(8,128)S(1)} %get-tuple-element.137, pred[]{:T(512)S(6)} %compare.19, bf16[512,128]{1,0:T(8,128)(2,1)S(1)} %dynamic-slice_bitcast_fusion.2), kind=kOutput, calls=%fused_computation.6.clone.1 | convolution fusion | flops 136577024 | bytes 5373953 | tf_op jit(solution)/shard_map/while/body/eval_jaxpr/dot_general | solution.py:90
  99.3 2.7 %fusion.72 = (f32[2048]{0:T(1024)S(1)}, f32[512,2048]{1,0:T(8,128)}) fusion(bf16[2048,64]{1,0:T(8,128)(2,1)S(1)} %get-tuple-element.147, bf16[512,128]{1,0:T(8,128)(2,1)S(1)} %dynamic-slice_bitcast_fusion.2), kind=kOutput, calls=%fused_computation.4.clone.1 | convolution fusion | flops 136312832 | bytes 4595712 | tf_op jit(solution)/shard_map/while/body/eval_jaxpr/qd,kd->qk/dot_general | solution.py:86
  101.9 3.1 %convolution_add_fusion.2 = f32[2048,64]{0,1:T(8,128)S(1)} fusion(f32[512,2048]{1,0:T(8,128)} %get-tuple-element.127, f32[2048,64]{0,1:T(8,128)S(1)} %get-tuple-element.137, pred[]{:T(512)S(6)} %compare.19, bf16[512,128]{1,0:T(8,128)(2,1)S(1)} %dynamic-slice_bitcast_fusion.2), kind=kOutput, calls=%fused_computation.6.clone.1 | convolution fusion | flops 136577024 | bytes 5373953 | tf_op jit(solution)/shard_map/while/body/eval_jaxpr/dot_general | solution.py:90
  105.0 2.7 %fusion.72 = (f32[2048]{0:T(1024)S(1)}, f32[512,2048]{1,0:T(8,128)}) fusion(bf16[2048,64]{1,0:T(8,128)(2,1)S(1)} %get-tuple-element.147, bf16[512,128]{1,0:T(8,128)(2,1)S(1)} %dynamic-slice_bitcast_fusion.2), kind=kOutput, calls=%fused_computation.4.clone.1 | convolution fusion | flops 136312832 | bytes 4595712 | tf_op jit(solution)/shard_map/while/body/eval_jaxpr/qd,kd->qk/dot_general | solution.py:86
  107.7 3.1 %convolution_add_fusion.2 = f32[2048,64]{0,1:T(8,128)S(1)} fusion(f32[512,2048]{1,0:T(8,128)} %get-tuple-element.127, f32[2048,64]{0,1:T(8,128)S(1)} %get-tuple-element.137, pred[]{:T(512)S(6)} %compare.19, bf16[512,128]{1,0:T(8,128)(2,1)S(1)} %dynamic-slice_bitcast_fusion.2), kind=kOutput, calls=%fused_computation.6.clone.1 | convolution fusion | flops 136577024 | bytes 5373953 | tf_op jit(solution)/shard_map/while/body/eval_jaxpr/dot_general | solution.py:90
  110.8 2.7 %fusion.72 = (f32[2048]{0:T(1024)S(1)}, f32[512,2048]{1,0:T(8,128)}) fusion(bf16[2048,64]{1,0:T(8,128)(2,1)S(1)} %get-tuple-element.147, bf16[512,128]{1,0:T(8,128)(2,1)S(1)} %dynamic-slice_bitcast_fusion.2), kind=kOutput, calls=%fused_computation.4.clone.1 | convolution fusion | flops 136312832 | bytes 4595712 | tf_op jit(solution)/shard_map/while/body/eval_jaxpr/qd,kd->qk/dot_general | solution.py:86
  113.5 3.1 %convolution_add_fusion.2 = f32[2048,64]{0,1:T(8,128)S(1)} fusion(f32[512,2048]{1,0:T(8,128)} %get-tuple-element.127, f32[2048,64]{0,1:T(8,128)S(1)} %get-tuple-element.137, pred[]{:T(512)S(6)} %compare.19, bf16[512,128]{1,0:T(8,128)(2,1)S(1)} %dynamic-slice_bitcast_fusion.2), kind=kOutput, calls=%fused_computation.6.clone.1 | convolution fusion | flops 136577024 | bytes 5373953 | tf_op jit(solution)/shard_map/while/body/eval_jaxpr/dot_general | solution.py:90
  116.7 2.7 %fusion.72 = (f32[2048]{0:T(1024)S(1)}, f32[512,2048]{1,0:T(8,128)}) fusion(bf16[2048,64]{1,0:T(8,128)(2,1)S(1)} %get-tuple-element.147, bf16[512,128]{1,0:T(8,128)(2,1)S(1)} %dynamic-slice_bitcast_fusion.2), kind=kOutput, calls=%fused_computation.4.clone.1 | convolution fusion | flops 136312832 | bytes 4595712 | tf_op jit(solution)/shard_map/while/body/eval_jaxpr/qd,kd->qk/dot_general | solution.py:86
  119.3 3.1 %convolution_add_fusion.2 = f32[2048,64]{0,1:T(8,128)S(1)} fusion(f32[512,2048]{1,0:T(8,128)} %get-tuple-element.127, f32[2048,64]{0,1:T(8,128)S(1)} %get-tuple-element.137, pred[]{:T(512)S(6)} %compare.19, bf16[512,128]{1,0:T(8,128)(2,1)S(1)} %dynamic-slice_bitcast_fusion.2), kind=kOutput, calls=%fused_computation.6.clone.1 | convolution fusion | flops 136577024 | bytes 5373953 | tf_op jit(solution)/shard_map/while/body/eval_jaxpr/dot_general | solution.py:90
  125.1 3.1 %convolution_add_fusion.2 = f32[2048,64]{0,1:T(8,128)S(1)} fusion(f32[512,2048]{1,0:T(8,128)} %get-tuple-element.127, f32[2048,64]{0,1:T(8,128)S(1)} %get-tuple-element.137, pred[]{:T(512)S(6)} %compare.19, bf16[512,128]{1,0:T(8,128)(2,1)S(1)} %dynamic-slice_bitcast_fusion.2), kind=kOutput, calls=%fused_computation.6.clone.1 | convolution fusion | flops 136577024 | bytes 5373953 | tf_op jit(solution)/shard_map/while/body/eval_jaxpr/dot_general | solution.py:90
  128.2 2.7 %fusion.72 = (f32[2048]{0:T(1024)S(1)}, f32[512,2048]{1,0:T(8,128)}) fusion(bf16[2048,64]{1,0:T(8,128)(2,1)S(1)} %get-tuple-element.147, bf16[512,128]{1,0:T(8,128)(2,1)S(1)} %dynamic-slice_bitcast_fusion.2), kind=kOutput, calls=%fused_computation.4.clone.1 | convolution fusion | flops 136312832 | bytes 4595712 | tf_op jit(solution)/shard_map/while/body/eval_jaxpr/qd,kd->qk/dot_general | solution.py:86
  130.9 3.1 %convolution_add_fusion.2 = f32[2048,64]{0,1:T(8,128)S(1)} fusion(f32[512,2048]{1,0:T(8,128)} %get-tuple-element.127, f32[2048,64]{0,1:T(8,128)S(1)} %get-tuple-element.137, pred[]{:T(512)S(6)} %compare.19, bf16[512,128]{1,0:T(8,128)(2,1)S(1)} %dynamic-slice_bitcast_fusion.2), kind=kOutput, calls=%fused_computation.6.clone.1 | convolution fusion | flops 136577024 | bytes 5373953 | tf_op jit(solution)/shard_map/while/body/eval_jaxpr/dot_general | solution.py:90
  137.3 5.4 %all-to-all-start.1 = ((bf16[8,48,512]{2,1,0:T(8,128)(2,1)}), bf16[8,48,512]{2,1,0:T(8,128)(2,1)S(1)}, u32[]{:S(2)}, u32[]{:S(2)}) async-start(bf16[8,48,512]{2,1,0:T(8,128)(2,1)} %reduce-scatter.5.cloned.1.call-done), calls=%async_computation.3 | async-start | bytes 786432 | tf_op jit(solution)/shard_map/all_to_all | solution.py:142
  142.7 27.9 %reduce-scatter.3.cloned.1.call-done = bf16[128,2048]{1,0:T(8,128)(2,1)} async-done(((bf16[512,2048]{1,0:T(8,128)(2,1)}), bf16[128,2048]{1,0:T(8,128)(2,1)}) %reduce-scatter.3.cloned.1.call-update) | async-done | bytes 524304 | tf_op jit(solution)/shard_map/reduce_scatter | solution.py:112
  (104 shorter events, 23.4 us)
Async XLA Ops:
  8.0 126.3 %copy-start = (bf16[256,2048]{1,0:T(8,128)(2,1)S(1)}, bf16[256,2048]{1,0:T(8,128)(2,1)}, u32[]{:S(2)}) copy-start(bf16[256,2048]{1,0:T(8,128)(2,1)} %param.21) | copy-start | bytes 3145732
  18.1 5.9 %copy-start.2 = (bf16[512,256]{1,0:T(8,128)(2,1)S(1)}, bf16[512,256]{1,0:T(8,128)(2,1)}, u32[]{:S(2)}) copy-start(bf16[512,256]{1,0:T(8,128)(2,1)} %param.18) | copy-start | bytes 786436
  18.2 5.9 %copy-start.3 = (bf16[512,256]{1,0:T(8,128)(2,1)S(1)}, bf16[512,256]{1,0:T(8,128)(2,1)}, u32[]{:S(2)}) copy-start(bf16[512,256]{1,0:T(8,128)(2,1)} %param.17) | copy-start | bytes 786436
  18.2 6.3 %copy-start.6 = (f32[64]{0:T(128)S(1)}, f32[64]{0:T(128)}, u32[]{:S(2)}) copy-start(f32[64]{0:T(128)} %param.20) | copy-start | bytes 772
  18.2 7.5 %copy-start.1 = (bf16[512,256]{1,0:T(8,128)(2,1)S(1)}, bf16[512,256]{1,0:T(8,128)(2,1)}, u32[]{:S(2)}) copy-start(bf16[512,256]{1,0:T(8,128)(2,1)} %param.16) | copy-start | bytes 786436
  18.2 58.1 %all-to-all-start = ((bf16[8,48,2048]{2,1,0:T(8,128)(2,1)}), bf16[8,48,2048]{2,1,0:T(8,128)(2,1)}, u32[]{:S(2)}, u32[]{:S(2)}) async-start(bf16[8,48,2048]{2,1,0:T(8,128)(2,1)} %bitcast.13), calls=%async_computation.1 | async-start | bytes 3145728 | tf_op jit(solution)/shard_map/all_to_all | solution.py:132
  24.0 2.2 %copy-start.7 = (f32[64]{0:T(128)S(1)}, f32[64]{0:T(128)}, u32[]{:S(2)}) copy-start(f32[64]{0:T(128)} %param.19) | copy-start | bytes 772
  24.0 50.6 %all-gather.2.cloned.1.call-start = ((), (), s32[]{:S(2)}) async-start(), calls=%async_computation.4 | async-start | bytes 1179648 | tf_op jit(solution)/shard_map/all_gather | solution.py:100
  25.6 111.7 %reduce-scatter.5.cloned.1.call-start = ((), (), s32[]{:S(2)}) async-start(), calls=%async_computation.6 | async-start | bytes 1966080 | tf_op jit(solution)/shard_map/reduce_scatter | solution.py:139
  76.2 4.6 %copy-start.8 = (bf16[1,2048,1024]{2,1,0:T(8,128)(2,1)S(1)}, bf16[1,2048,1024]{2,1,0:T(8,128)(2,1)}, u32[]{:S(2)}) copy-start(bf16[1,2048,1024]{2,1,0:T(8,128)(2,1)} %param.28) | copy-start | bytes 12582916
  80.9 3.6 %copy-start.9 = (bf16[1,1024,2048]{2,1,0:T(8,128)(2,1)S(1)}, bf16[1,1024,2048]{2,1,0:T(8,128)(2,1)}, u32[]{:S(2)}) copy-start(bf16[1,1024,2048]{2,1,0:T(8,128)(2,1)} %param.29) | copy-start | bytes 12582916
  87.5 83.2 %reduce-scatter.3.cloned.1.call-start = ((), (), s32[]{:S(2)}) async-start(), calls=%async_computation.5 | async-start | bytes 2621440 | tf_op jit(solution)/shard_map/reduce_scatter | solution.py:112
  136.4 0.7 copy-start.4
  136.4 35.5 %copy-start.5 = (f32[2048]{0:T(1024)S(1)}, f32[2048]{0:T(1024)}, u32[]{:S(2)}) copy-start(f32[2048]{0:T(1024)} %param.22) | copy-start | bytes 24580
  137.3 36.6 %all-to-all-start.1 = ((bf16[8,48,512]{2,1,0:T(8,128)(2,1)}), bf16[8,48,512]{2,1,0:T(8,128)(2,1)S(1)}, u32[]{:S(2)}, u32[]{:S(2)}) async-start(bf16[8,48,512]{2,1,0:T(8,128)(2,1)} %reduce-scatter.5.cloned.1.call-done), calls=%async_computation.3 | async-start | bytes 786432 | tf_op jit(solution)/shard_map/all_to_all | solution.py:142
Sparse Core Ops, SparseCore 0:
  27.4 47.1 all-gather.1
Sparse Core Ops, SparseCore 1:
  87.5 30.8 reduce-scatter.4
  136.5 34.1 reduce-scatter.2
where the time goes:
time: 187 us; the launch traced here: 184 us
  waiting for transfers between devices  75.9 us (41%)
  matrix products  59.2 us (32%)
  between operations  15.8 us (8%)
  starting transfers between devices  11.3 us (6%)
  local copies, waits for them, and re-layouts  11.2 us (6%)
  other arithmetic  10.4 us (6%)
    all_gather x1, waiting for transfers between devices, mixer_half(): gathered_piece = lax.all_gather(paired, 'ep', axis=0, tiled=True)  47.9 us
    reduce_scatter x1, waiting for transfers between devices, mixer_half(): lax.psum_scatter(jnp.dot(head_out, w_out, preferred_element_type=jnp.floa...  27.9 us
    dot_general x8, matrix products, attend_block(): jnp.dot(weights.astype(jnp.bfloat16), block_values, preferred_element_typ...  24.8 us
    dot_general x8, matrix products, attend_block(): jnp.einsum('qd,kd->qk', query_rows, block_keys, preferred_element_type=jn...  21.2 us
    all_to_all x1, starting transfers between devices, experts_half(): lax.all_to_all(outgoing, 'ep', split_axis=0, concat_axis=0, tiled=True)  5.83 us
    all_to_all x1, starting transfers between devices, experts_half(): lax.all_to_all(summed, 'ep', split_axis=0, concat_axis=0, tiled=True)  5.37 us
    dot_general x1, matrix products, experts_half(): gate_pre = jnp.dot(arrived, w_gate[0], preferred_element_type=jnp.float32)  4.59 us
    unnamed x26, local copies, waits for them, and re-layouts  3.79 us
  transfers between devices with their start and end apart: 5, of which 2 were waited for; matrix products, arithmetic and copies ran while one was open for 30% of the time, Pallas kernels for 0%

commit v1 on v0

v1 whole, which is shorter than its diff:
```python
import functools

import jax
import jax.numpy as jnp
from jax import lax
from jax.experimental import pallas as pl
from jax.experimental.pallas import tpu as pltpu
from jax.sharding import PartitionSpec as P

GRID_W = 128
EPSILON = 1e-06
ROPE_BASE = 10000.0
MESH = pl.DeviceIdType.MESH


def head_norm(values, gain):
    return values * lax.rsqrt(jnp.mean(values * values, axis=-1, keepdims=True) + EPSILON) * gain


def rotate_half(values, angles):
    quarter = angles.shape[-1]
    first_part = values[..., :quarter]
    second_part = values[..., quarter:]
    cosine = jnp.cos(angles)[:, None, :]
    sine_part = jnp.sin(angles)[:, None, :]
    return jnp.concatenate(
        [
            first_part * cosine - second_part * sine_part,
            second_part * cosine + first_part * sine_part,
        ],
        axis=-1,
    )


def grid_rotary(values, offset):
    row_count = values.shape[0]
    head_width = values.shape[-1]
    quarter = head_width // 4
    half_width = head_width // 2
    position = offset + jnp.arange(row_count, dtype=jnp.int32)
    grid_row = (position // GRID_W).astype(jnp.float32)
    grid_col = (position % GRID_W).astype(jnp.float32)
    inverse = ROPE_BASE ** (-jnp.arange(quarter, dtype=jnp.float32) / quarter)
    return jnp.concatenate(
        [
            rotate_half(values[..., :half_width], grid_row[:, None] * inverse[None, :]),
            rotate_half(values[..., half_width:], grid_col[:, None] * inverse[None, :]),
        ],
        axis=-1,
    )


def kernel(
    dims,
    q_ref, pair_ref, outgo_ref, mixw_ref, wout_ref, gain_ref, wg_hbm, wu_hbm, wd_hbm,
    attn_ref, moe_ref,
    wg, wu, wd, kvbuf, vx, acc, arrived, hidden,
    pa, pa_in, pa_red, pa_in2, pm, pm_in, pm_red, pm_in2, summed, ret,
    w_sem, loc_sem, kv_s, kv_r, disp_s, disp_r, rel_s, rel_r, fwd_s,
    a1_s, a1_r, a2_s, a2_r, m1_s, m1_r, m2_s, m2_r, ret_s, ret_r,
):
    n_ep, n_tp, heads, cap = dims
    ny = n_tp // 2
    ep = lax.axis_index("ep")
    tp = lax.axis_index("tp")
    core = lax.rem(tp, 2)
    row = tp // 2
    partner = row * 2 + 1 - core
    rows_kv = pair_ref.shape[0]
    dq = outgo_ref.shape[1]
    slots = outgo_ref.shape[0]
    piece = attn_ref.shape[0]

    def remote(src, dst, ss, rs, e, t):
        return pltpu.make_async_remote_copy(
            src_ref=src, dst_ref=dst, send_sem=ss, recv_sem=rs,
            device_id=(e, t), device_id_type=MESH,
        )

    def ep_at(d):
        return lax.rem(ep + d, n_ep)

    def ep_from(d):
        return lax.rem(ep - d + n_ep, n_ep)

    def same_core(d):
        return lax.rem(row + d, ny) * 2 + core

    def row_from(d):
        return lax.rem(row - d + ny, ny)

    def slot_rows(e):
        return pl.ds(pl.multiple_of(e * cap, cap), cap)

    loads = [
        pltpu.make_async_copy(src, dst, w_sem.at[i])
        for i, (src, dst) in enumerate(((wg_hbm, wg), (wu_hbm, wu), (wd_hbm, wd)))
    ]
    own = pltpu.make_async_copy(
        outgo_ref.at[slot_rows(ep)], arrived.at[tp, slot_rows(ep)], loc_sem.at[0]
    )
    own.start()
    barrier = pltpu.get_barrier_semaphore()
    for d in range(1, n_ep):
        pl.semaphore_signal(barrier, inc=1, device_id=(ep_at(d), tp), device_id_type=MESH)
    for d in range(1, ny):
        pl.semaphore_signal(barrier, inc=1, device_id=(ep, same_core(d)), device_id_type=MESH)
    pl.semaphore_signal(barrier, inc=1, device_id=(ep, partner), device_id_type=MESH)
    pl.semaphore_wait(barrier, n_ep - 1 + ny - 1 + 1)

    disp = [
        remote(outgo_ref.at[slot_rows(ep_at(d))], arrived.at[tp, slot_rows(ep)],
               disp_s.at[d], disp_r.at[d], ep_at(d), tp)
        for d in range(1, n_ep)
    ]
    for copy in disp:
        copy.start()

    def kv_copy(d):
        return remote(pair_ref, kvbuf.at[ep], kv_s.at[d], kv_r.at[d], ep_at(d), tp)

    for d in range(1, n_ep):
        kv_copy(d).start()
    for copy in loads:
        copy.start()

    q_rows = q_ref.shape[0]
    tile = min(256, q_rows)

    def attend(keys_of, first):
        keys = keys_of[...]
        lanes = lax.broadcasted_iota(jnp.int32, keys.shape, 1)
        vx[...] = jnp.where(lanes < keys.shape[1] // 2, jnp.ones_like(keys), keys)

        def one(i, carry):
            for sub in range(2):
                at = pl.ds(pl.multiple_of(i * 2 * tile + sub * tile, tile), tile)
                scores = lax.dot_general(
                    q_ref[at, :], keys_of[...], (((1,), (1,)), ((), ())),
                    preferred_element_type=jnp.float32,
                )
                weights = jnp.exp(scores).astype(jnp.bfloat16)
                term = jnp.dot(weights, vx[...], preferred_element_type=jnp.float32)
                if first:
                    acc[at, :] = term
                else:
                    acc[at, :] += term
            return carry

        lax.fori_loop(0, q_rows // (2 * tile), one, 0)

    attend(pair_ref, True)

    def later(d, carry):
        kv_copy(d).wait_recv()
        attend(kvbuf.at[ep_from(d)], False)
        return carry

    early = max(1, n_ep * 3 // 8)
    late = max(early + 1, n_ep - 1)
    lax.fori_loop(1, early, later, 0)

    own.wait()
    for copy in disp:
        copy.wait_recv()
    relay = [
        remote(arrived.at[tp], arrived.at[tp], rel_s.at[d], rel_r.at[d], ep, same_core(d))
        for d in range(1, ny)
    ]
    cross = [
        remote(arrived.at[row_from(d) * 2 + core], arrived.at[row_from(d) * 2 + core],
               fwd_s.at[d], rel_r.at[ny + d], ep, partner)
        for d in range(ny)
    ]
    for copy in relay:
        copy.start()
    cross[0].start()
    lax.fori_loop(early, late, later, 0)
    for d in range(1, ny):
        relay[d - 1].wait_recv()
        cross[d].start()
    lax.fori_loop(late, n_ep, later, 0)

    outs = []
    tokens = q_rows // heads
    half = acc.shape[1] // 2
    for j in range(n_tp):
        pieces = []
        for h in range(heads):
            a = acc[h * tokens + j * piece : h * tokens + (j + 1) * piece, :]
            pieces.append((a[:, half:] / a[:, :half]).astype(jnp.bfloat16))
        mine = pieces[0] if heads == 1 else jnp.concatenate(pieces, axis=1)
        pa[j % 2, j // 2] = jnp.dot(
            mine, wout_ref[...], preferred_element_type=jnp.float32
        ).astype(jnp.bfloat16)
    a1 = remote(pa.at[1 - core], pa_in, a1_s.at[0], a1_r.at[0], ep, partner)
    a1.start()

    for copy in cross:
        copy.wait_recv()
    loads[0].wait()
    loads[1].wait()
    a1.wait_recv()
    for y in range(ny):
        pa_red[y] = (
            pa[core, y].astype(jnp.float32) + pa_in[y].astype(jnp.float32)
        ).astype(jnp.bfloat16)
    a2 = [
        remote(pa_red.at[lax.rem(row + d, ny)], pa_in2.at[row],
               a2_s.at[d], a2_r.at[d], ep, same_core(d))
        for d in range(1, ny)
    ]
    for copy in a2:
        copy.start()

    ff = hidden.shape[1]
    step = min(256, ff)

    def gated(i, carry):
        at = pl.ds(pl.multiple_of(i * step, step), step)
        gate = jnp.zeros((slots, step), jnp.float32)
        up = jnp.zeros((slots, step), jnp.float32)
        for q in range(n_tp):
            x = arrived[q]
            gate = gate + jnp.dot(x, wg[q * dq : (q + 1) * dq, at], preferred_element_type=jnp.float32)
            up = up + jnp.dot(x, wu[q * dq : (q + 1) * dq, at], preferred_element_type=jnp.float32)
        hidden[:, at] = (gate / (1.0 + jnp.exp(-gate)) * up).astype(jnp.bfloat16)
        return carry

    lax.fori_loop(0, ff // step, gated, 0)
    loads[2].wait()

    def down_for(which):
        def down(y, carry):
            cols = pl.ds(pl.multiple_of((y * 2 + which) * dq, dq), dq)
            pm[which, y] = jnp.dot(
                hidden[...], wd[:, cols], preferred_element_type=jnp.float32
            ).astype(jnp.bfloat16)
            return carry

        lax.fori_loop(0, ny, down, 0)

    m1 = remote(pm.at[1 - core], pm_in, m1_s.at[0], m1_r.at[0], ep, partner)
    down_for(1 - core)
    m1.start()
    down_for(core)
    m1.wait_recv()
    for y in range(ny):
        pm_red[y] = (
            pm[core, y].astype(jnp.float32) + pm_in[y].astype(jnp.float32)
        ).astype(jnp.bfloat16)
    m2 = [
        remote(pm_red.at[lax.rem(row + d, ny)], pm_in2.at[row],
               m2_s.at[d], m2_r.at[d], ep, same_core(d))
        for d in range(1, ny)
    ]
    for copy in m2:
        copy.start()

    for copy in a2:
        copy.wait_recv()
    mixed = pa_red[row].astype(jnp.float32)
    for d in range(1, ny):
        mixed = mixed + pa_in2[row_from(d)].astype(jnp.float32)
    square = jnp.mean(mixed * mixed, axis=-1, keepdims=True)
    attn_ref[...] = (mixed * lax.rsqrt(square + EPSILON) * gain_ref[...]).astype(jnp.bfloat16)

    for copy in m2:
        copy.wait_recv()
    total = pm_red[row].astype(jnp.float32)
    for d in range(1, ny):
        total = total + pm_in2[row_from(d)].astype(jnp.float32)
    summed[...] = total.astype(jnp.bfloat16)
    back = [
        remote(summed.at[slot_rows(ep_at(d))], ret.at[slot_rows(ep)],
               ret_s.at[d], ret_r.at[d], ep_at(d), tp)
        for d in range(1, n_ep)
    ]
    for copy in back:
        copy.start()
    mine = pltpu.make_async_copy(
        summed.at[slot_rows(ep)], ret.at[slot_rows(ep)], loc_sem.at[1]
    )
    mine.start()
    mine.wait()
    for copy in back:
        copy.wait_recv()
    mixw = mixw_ref[...]
    high = mixw.astype(jnp.bfloat16)
    low = (mixw - high.astype(jnp.float32)).astype(jnp.bfloat16)
    moe_ref[...] = (
        jnp.dot(high, ret[...], preferred_element_type=jnp.float32)
        + jnp.dot(low, ret[...], preferred_element_type=jnp.float32)
    ).astype(jnp.bfloat16)

    for copy in disp + relay + cross + [a1] + a2 + [m1] + m2 + back:
        copy.wait_send()

    def kv_done(d, carry):
        kv_copy(d).wait_send()
        return carry

    lax.fori_loop(1, n_ep, kv_done, 0)


def per_device(
    n_ep, n_tp,
    q_in, k_in, v_in, q_gain, k_gain, w_out, post_gain,
    moe_in, routes, route_logits, pre_gain, w_gate, w_up, w_down,
):
    bf16 = jnp.bfloat16
    head = q_gain.shape[0]
    rows = q_in.shape[0]
    heads = q_in.shape[1] // head
    kv_count = k_in.shape[1] // head
    repeat = heads * n_tp // kv_count
    ny = n_tp // 2
    offset = lax.axis_index("ep") * rows
    queries = head_norm(q_in.astype(jnp.float32).reshape(rows, heads, head), q_gain)
    queries = grid_rotary(queries, offset).astype(bf16) * jnp.asarray(head ** (-0.5), bf16)
    queries = jnp.transpose(queries, (1, 0, 2)).reshape(heads * rows, head)
    queries = jnp.concatenate([queries, jnp.zeros_like(queries)], axis=1)
    kv_index = lax.axis_index("tp") * heads // repeat
    keys = lax.dynamic_slice_in_dim(k_in, kv_index * head, head, 1)
    values = lax.dynamic_slice_in_dim(v_in, kv_index * head, head, 1)
    keys = head_norm(keys.astype(jnp.float32)[:, None, :], k_gain)
    keys = grid_rotary(keys, offset)[:, 0, :].astype(bf16)
    paired = jnp.concatenate([keys, values], axis=1)

    tokens, top = routes.shape
    width = moe_in.shape[1]
    dq = width // n_tp
    need = max(2, 3 * top * tokens // (2 * n_ep))
    cap = -(-need // 16) * 16
    slots = n_ep * cap
    x = moe_in.astype(jnp.float32)
    scale = lax.rsqrt(jnp.mean(x * x, axis=-1, keepdims=True) + EPSILON)
    first = lax.axis_index("tp") * dq
    x = lax.dynamic_slice_in_dim(moe_in, first, dq, 1).astype(jnp.float32)
    normed = (x * scale * lax.dynamic_slice_in_dim(pre_gain, first, dq, 0)).astype(bf16)
    slot = jnp.arange(slots, dtype=jnp.int32)[None, :]
    route_weight = jax.nn.softmax(route_logits, axis=-1)
    named = jnp.zeros((tokens, slots), jnp.bool_)
    share = jnp.zeros((tokens, slots), jnp.float32)
    for j in range(top):
        hit = routes[:, j : j + 1] == slot // cap
        named = named | hit
        share = share + jnp.where(hit, route_weight[:, j : j + 1], 0.0)
    earlier = jnp.tril(jnp.ones((tokens, tokens), bf16), -1)
    rank = jnp.dot(earlier, named.astype(bf16), preferred_element_type=jnp.float32)
    placed = named & (rank == (slot % cap).astype(jnp.float32))
    mixw = jnp.where(placed, share, 0.0)
    outgo = lax.dot_general(
        placed.astype(bf16), normed, (((0,), (0,)), ((), ())),
        preferred_element_type=jnp.float32,
    ).astype(bf16)

    piece = rows // n_tp
    ff = w_gate.shape[2]
    dma = pltpu.SemaphoreType.DMA
    vmem = pl.BlockSpec(memory_space=pltpu.VMEM)
    hbm = pl.BlockSpec(memory_space=pl.ANY)
    return pl.pallas_call(
        functools.partial(kernel, (n_ep, n_tp, heads, cap)),
        out_shape=(
            jax.ShapeDtypeStruct((piece, width), bf16),
            jax.ShapeDtypeStruct((tokens, dq), bf16),
        ),
        in_specs=[vmem] * 6 + [hbm] * 3,
        out_specs=(vmem, vmem),
        scratch_shapes=[
            pltpu.VMEM((width, ff), bf16),
            pltpu.VMEM((width, ff), bf16),
            pltpu.VMEM((ff, width), bf16),
            pltpu.VMEM((n_ep, rows, 2 * head), bf16),
            pltpu.VMEM((rows, 2 * head), bf16),
            pltpu.VMEM((heads * rows, 2 * head), jnp.float32),
            pltpu.VMEM((n_tp, slots, dq), bf16),
            pltpu.VMEM((slots, ff), bf16),
            pltpu.VMEM((2, ny, piece, width), bf16),
            pltpu.VMEM((ny, piece, width), bf16),
            pltpu.VMEM((ny, piece, width), bf16),
            pltpu.VMEM((ny, piece, width), bf16),
            pltpu.VMEM((2, ny, slots, dq), bf16),
            pltpu.VMEM((ny, slots, dq), bf16),
            pltpu.VMEM((ny, slots, dq), bf16),
            pltpu.VMEM((ny, slots, dq), bf16),
            pltpu.VMEM((slots, dq), bf16),
            pltpu.VMEM((slots, dq), bf16),
            dma((3,)), dma((2,)),
            dma((n_ep,)), dma((n_ep,)), dma((n_ep,)), dma((n_ep,)),
            dma((ny,)), dma((2 * ny,)), dma((ny,)),
            dma((1,)), dma((1,)), dma((ny,)), dma((ny,)),
            dma((1,)), dma((1,)), dma((ny,)), dma((ny,)),
            dma((n_ep,)), dma((n_ep,)),
        ],
        compiler_params=pltpu.CompilerParams(
            collective_id=0, has_side_effects=True, vmem_limit_bytes=60 * 1024 * 1024
        ),
    )(queries, paired, outgo, mixw, w_out, post_gain[None, :], w_gate[0], w_up[0], w_down[0])


def solution(mesh):
    return jax.shard_map(
        functools.partial(per_device, mesh.shape["ep"], mesh.shape["tp"]),
        mesh=mesh,
        in_specs=(
            P("ep", "tp"),
            P("ep", None),
            P("ep", None),
            P(),
            P(),
            P("tp", None),
            P(),
            P("ep", None),
            P("ep", None),
            P("ep", None),
            P(),
            P("ep", None, "tp"),
            P("ep", None, "tp"),
            P("ep", "tp", None),
        ),
        out_specs=(P(("ep", "tp"), None), P("ep", "tp")),
        check_vma=False,
    )
```

time: 187 us -> 103 us (0.55); the launches traced: 184 us -> 102 us
  Pallas kernels: 0 us -> 82.5 us
  waiting for transfers between devices: 75.9 us -> 0 us
  matrix products: 59.2 us -> 2.96 us
  between operations: 15.8 us -> 0.8 us
  starting transfers between devices: 11.3 us -> 0 us
  local copies, waits for them, and re-layouts: 11.2 us -> 6.42 us
    pallas_call x0 -> x1, Pallas kernels: none -> 82.5 us  [per_device(): pl.pallas_call(functools.partial(kernel, (n_ep, n_tp, heads, cap)), out_s...]
    dot_general x20 -> x2, matrix products: 59.2 us -> 2.96 us  [the longest x1 2.01 us: per_device(): lax.dot_general(placed.astype(bf16), normed, (((0,), (0,)), ((), ())), pr...]
    all_gather x1 -> x0, waiting for transfers between devices: 47.9 us -> none  [mixer_half(): gathered_piece = lax.all_gather(paired, 'ep', axis=0, tiled=True)]
    reduce_scatter x2 -> x0, waiting for transfers between devices: 28 us -> none  [the longest x1 27.9 us: mixer_half(): lax.psum_scatter(jnp.dot(head_out, w_out, preferred_element_type=jnp.floa...]
    all_to_all x2 -> x0, starting transfers between devices: 11.2 us -> none  [the longest x1 5.83 us: experts_half(): lax.all_to_all(outgoing, 'ep', split_axis=0, concat_axis=0, tiled=True)]
    gather x2 -> x0, local copies, waits for them, and re-layouts: 4.28 us -> none  [the longest x1 3.13 us: experts_half(): padded[slot_owner // top_count].reshape(expert_count, capacity, model_width)]
    convert_element_type x5 -> x1, other arithmetic: 3.32 us -> 0.19 us  [per_device(): keys = grid_rotary(keys, offset)[:, 0, :].astype(bf16)]
    unnamed x26 -> x9, local copies, waits for them, and re-layouts: 3.79 us -> 3.61 us
  transfers between devices with their start and end apart: 5 -> 0, of which waited for: 2 -> 0; matrix products, arithmetic and copies ran while one was open for 30% -> 0% of each run, Pallas kernels for 0% -> 0%
where the time goes in v1:
time: 103 us; the launch traced here: 102 us
  Pallas kernels  82.5 us (80%)
  other arithmetic  9.62 us (9%)
  local copies, waits for them, and re-layouts  6.42 us (6%)
  matrix products  2.96 us (3%)
    pallas_call x1, Pallas kernels, per_device(): pl.pallas_call(functools.partial(kernel, (n_ep, n_tp, heads, cap)), out_s...  82.5 us
    unnamed x9, local copies, waits for them, and re-layouts  3.61 us
    another operation x2, other arithmetic  2.48 us

profile of v1, /device:TPU:9, one launch (start us, length us, event | category | flops | bytes accessed | tf_op | source)
XLA Modules:
  0.0 102.3 jit_solution(15908171862697558299)
XLA Ops:
  0.7 0.8 reduce_max.9
  1.5 0.7 fusion.51
  2.2 0.7 fusion.50
  2.9 1.2 %multiply_reduce_fusion = f32[128]{0:T(128)S(1)} fusion(bf16[128,2048]{1,0:T(8,128)(2,1)} %param.21), kind=kLoop, calls=%fused_computation.3 | loop fusion | flops 786304 | bytes 524800 | tf_op jit(solution)/shard_map/reduce_sum | solution.py:337
  4.1 0.8 slice_bitcast_fusion.3
  4.9 0.8 dynamic_slice.15
  5.6 1.1 %fusion.11 = f32[512]{0:T(512)S(1)} fusion(bf16[512,256]{1,0:T(8,128)(2,1)} %param.15, s32[]{:T(128)S(6)} %select_n.77), kind=kLoop, calls=%fused_computation.22 | loop fusion | flops 97792 | bytes 67588 | tf_op jit(solution)/shard_map/reduce_sum | solution.py:17
  6.8 0.1 constant_dynamic-slice_fusion
  6.9 0.3 multiply_cosine_fusion.3
  7.2 1.0 fusion.24
  8.2 1.1 %fusion.13 = f32[512,1,64]{2,0,1:T(8,128)S(1)} fusion(f32[64]{0:T(128)} %param.18, f32[512]{0:T(512)S(1)} %add_rsqrt_fusion.1, bf16[512,256]{1,0:T(8,128)(2,1)} %param.15, s32[]{:T(128)S(6)} %select_n.77), kind=kLoop, calls=%fused_computation.24 | loop fusion | flops 98304 | bytes 198916 | tf_op jit(solution)/shard_map/mul | solution.py:17
  9.3 2.4 %fusion.19 = (bf16[512,1,16]{2,0,1:T(8,128)(2,1)S(1)}, bf16[512,1,16]{2,0,1:T(8,128)(2,1)S(1)}, bf16[512,1,16]{2,0,1:T(8,128)(2,1)S(1)}, bf16[512,1,16]{2,0,1:T(8,128)(2,1)S(1)}) fusion(f32[512,1,64]{2,0,1:T(8,128)S(1)} %fusion.13, f32[512]{0:T(512)S(1)} %get-tuple-element.26, f32[16]{0:T(128)S(1)} %multiply_power_fusion, f32[512]{0:T(512)S(1)} %get-tuple-element.27), kind=kLoop, calls=%fused_computation.30 | loop fusion | flops 147456 | bytes 200768 | tf_op jit(solution)/shard_map/convert.1
  11.7 0.2 maximum_bitcast_fusion
  11.9 0.8 pad_maximum_fusion.pair_ref
  12.6 0.1 copy.19
  12.8 0.1 fusion.1
  12.9 0.1 fusion.2
  13.0 0.1 subtract_convert_fusion.1
  13.2 0.3 copy.20
  13.4 0.9 concatenate.15.q_ref
  14.3 2.0 %convolution_convert_fusion.outgo_ref = bf16[384,512]{1,0:T(8,128)(2,1)} fusion(pred[128,384]{1,0:T(32,128)(4,1)S(1)} %get-tuple-element.25, f32[512]{0:T(512)S(1)} %dynamic_slice.15, f32[128]{0:T(128)S(1)} %add_rsqrt_fusion.2, bf16[128,2048]{1,0:T(8,128)(2,1)} %param.21, s32[]{:T(128)S(6)} %select_n.81), kind=kOutput, calls=%fused_computation | convolution fusion | flops 50790400 | bytes 576004 | tf_op jit(solution)/shard_map/dot_general | solution.py:353
  16.3 82.5 %shard_map.149 = (bf16[128,2048]{1,0:T(8,128)(2,1)}, bf16[128,512]{1,0:T(8,128)(2,1)}) custom-call(bf16[2048,128]{1,0:T(8,128)(2,1)} %concatenate.15.q_ref, bf16[512,128]{1,0:T(8,128)(2,1)} %pad_maximum_fusion.pair_ref, bf16[384,512]{1,0:T(8,128)(2,1)} %convolution_convert_fusion.outgo_ref, f32[128,384]{1,0:T(8,128)} %get-tuple-element.24.mixw_ref, ...), custom_call_target="tpu_custom_call" | custom-call | tf_op jit(solution)/shard_map/pallas_call | solution.py:363
  98.8 1.9 %copy.27 = bf16[128,2048]{1,0:T(8,128)(2,1)} copy(bf16[128,2048]{1,0:T(8,128)(2,1)} %get-tuple-element.32) | data formatting | bytes 1048576
  100.7 1.6 %copy.28 = bf16[128,512]{1,0:T(8,128)(2,1)} copy(bf16[128,512]{1,0:T(8,128)(2,1)} %get-tuple-element.33) | data formatting | bytes 262144
  (15 shorter events, 0.1 us)
Async XLA Ops:
  0.6 6.2 %copy-start = (bf16[512,256]{1,0:T(8,128)(2,1)S(1)}, bf16[512,256]{1,0:T(8,128)(2,1)}, u32[]{:S(2)}) copy-start(bf16[512,256]{1,0:T(8,128)(2,1)} %param.16) | copy-start | bytes 786436
  0.6 12.2 %copy-start.2 = (f32[64]{0:T(128)S(1)}, f32[64]{0:T(128)}, u32[]{:S(2)}) copy-start(f32[64]{0:T(128)} %param.17) | copy-start | bytes 772
  0.7 12.0 %copy-start.1 = (bf16[512,256]{1,0:T(8,128)(2,1)S(1)}, bf16[512,256]{1,0:T(8,128)(2,1)}, u32[]{:S(2)}) copy-start(bf16[512,256]{1,0:T(8,128)(2,1)} %param.14) | copy-start | bytes 786436

commit v2 on v1

--- a/solution.py
+++ b/solution.py
@@ -52,9 +52,9 @@
 
 def kernel(
     dims,
-    q_ref, pair_ref, outgo_ref, mixw_ref, wout_ref, gain_ref, wg_hbm, wu_hbm, wd_hbm,
+    q_ref, pair_ref, x_ref, route_ref, logit_ref, pre_ref, ids_ref, wout_ref, gain_ref, wg_hbm, wu_hbm, wd_hbm,
     attn_ref, moe_ref,
-    wg, wu, wd, kvbuf, vx, acc, arrived, hidden,
+    outgo_ref, mixw_ref, wg, wu, wd, kvbuf, vx, acc, arrived, hidden,
     pa, pa_in, pa_red, pa_in2, pm, pm_in, pm_red, pm_in2, summed, ret,
     w_sem, loc_sem, kv_s, kv_r, disp_s, disp_r, rel_s, rel_r, fwd_s,
     a1_s, a1_r, a2_s, a2_r, m1_s, m1_r, m2_s, m2_r, ret_s, ret_r,
@@ -96,16 +96,45 @@
         pltpu.make_async_copy(src, dst, w_sem.at[i])
         for i, (src, dst) in enumerate(((wg_hbm, wg), (wu_hbm, wu), (wd_hbm, wd)))
     ]
-    own = pltpu.make_async_copy(
-        outgo_ref.at[slot_rows(ep)], arrived.at[tp, slot_rows(ep)], loc_sem.at[0]
-    )
-    own.start()
     barrier = pltpu.get_barrier_semaphore()
     for d in range(1, n_ep):
         pl.semaphore_signal(barrier, inc=1, device_id=(ep_at(d), tp), device_id_type=MESH)
     for d in range(1, ny):
         pl.semaphore_signal(barrier, inc=1, device_id=(ep, same_core(d)), device_id_type=MESH)
     pl.semaphore_signal(barrier, inc=1, device_id=(ep, partner), device_id_type=MESH)
+
+    x = x_ref[...].astype(jnp.float32)
+    scale = lax.rsqrt(jnp.mean(x * x, axis=-1, keepdims=True) + EPSILON)
+    mine = pl.ds(pl.multiple_of(tp * dq, dq), dq)
+    normed = (x_ref[:, mine].astype(jnp.float32) * scale * pre_ref[:, mine]).astype(jnp.bfloat16)
+    logits = logit_ref[...]
+    top = logits.shape[1]
+    tokens = logits.shape[0]
+    power = jnp.exp(logits - jnp.max(logits, axis=1, keepdims=True))
+    chance = power / jnp.sum(power, axis=1, keepdims=True)
+    named = jnp.zeros((tokens, slots), jnp.float32)
+    share = jnp.zeros((tokens, slots), jnp.float32)
+    for j in range(top):
+        hit = route_ref[:, j : j + 1] == ids_ref[0:1, :]
+        named = jnp.where(hit, 1.0, named)
+        share = jnp.where(hit, chance[:, j : j + 1], share)
+    below = lax.broadcasted_iota(jnp.int32, (tokens, tokens), 1) < lax.broadcasted_iota(
+        jnp.int32, (tokens, tokens), 0
+    )
+    rank = jnp.dot(
+        jnp.where(below, 1.0, 0.0).astype(jnp.bfloat16), named.astype(jnp.bfloat16),
+        preferred_element_type=jnp.float32,
+    )
+    placed = jnp.where(rank == ids_ref[1:2, :].astype(jnp.float32), named, 0.0)
+    mixw_ref[...] = placed * share
+    outgo_ref[...] = lax.dot_general(
+        placed.astype(jnp.bfloat16), normed, (((0,), (0,)), ((), ())),
+        preferred_element_type=jnp.float32,
+    ).astype(jnp.bfloat16)
+    own = pltpu.make_async_copy(
+        outgo_ref.at[slot_rows(ep)], arrived.at[tp, slot_rows(ep)], loc_sem.at[0]
+    )
+    own.start()
     pl.semaphore_wait(barrier, n_ep - 1 + ny - 1 + 1)
 
     disp = [
@@ -113,14 +142,28 @@
                disp_s.at[d], disp_r.at[d], ep_at(d), tp)
         for d in range(1, n_ep)
     ]
+    nz = n_ep // 2
+    side = lax.rem(ep, 2)
+    col = ep // 2
+    mate = col * 2 + 1 - side
+
+    def col_from(d, which):
+        return lax.rem(col - d + nz, nz) * 2 + which
+
+    def kv_direct(d):
+        return remote(pair_ref, kvbuf.at[ep], kv_s.at[d], kv_r.at[d],
+                      lax.rem(col + d, nz) * 2 + side, tp)
+
+    def kv_pass(d):
+        held = kvbuf.at[col_from(d, side)]
+        return remote(held, held, kv_s.at[nz + d], kv_r.at[nz + d], mate, tp)
+
+    kv_mate = remote(pair_ref, kvbuf.at[ep], kv_s.at[nz], kv_r.at[nz], mate, tp)
+    kv_mate.start()
     for copy in disp:
         copy.start()
-
-    def kv_copy(d):
-        return remote(pair_ref, kvbuf.at[ep], kv_s.at[d], kv_r.at[d], ep_at(d), tp)
-
-    for d in range(1, n_ep):
-        kv_copy(d).start()
+    for d in range(1, nz):
+        kv_direct(d).start()
     for copy in loads:
         copy.start()
 
@@ -151,13 +194,19 @@
 
     attend(pair_ref, True)
 
+    kv_mate.wait_recv()
+    attend(kvbuf.at[mate], False)
+
     def later(d, carry):
-        kv_copy(d).wait_recv()
-        attend(kvbuf.at[ep_from(d)], False)
+        kv_direct(d).wait_recv()
+        kv_pass(d).start()
+        attend(kvbuf.at[col_from(d, side)], False)
+        kv_pass(d).wait_recv()
+        attend(kvbuf.at[col_from(d, 1 - side)], False)
         return carry
 
-    early = max(1, n_ep * 3 // 8)
-    late = max(early + 1, n_ep - 1)
+    early = 1 + (nz - 1) // 3
+    late = max(early, nz - 1)
     lax.fori_loop(1, early, later, 0)
 
     own.wait()
@@ -179,7 +228,7 @@
     for d in range(1, ny):
         relay[d - 1].wait_recv()
         cross[d].start()
-    lax.fori_loop(late, n_ep, later, 0)
+    lax.fori_loop(late, nz, later, 0)
 
     outs = []
     tokens = q_rows // heads
@@ -293,14 +342,15 @@
         + jnp.dot(low, ret[...], preferred_element_type=jnp.float32)
     ).astype(jnp.bfloat16)
 
-    for copy in disp + relay + cross + [a1] + a2 + [m1] + m2 + back:
+    for copy in [kv_mate] + disp + relay + cross + [a1] + a2 + [m1] + m2 + back:
         copy.wait_send()
 
     def kv_done(d, carry):
-        kv_copy(d).wait_send()
+        kv_direct(d).wait_send()
+        kv_pass(d).wait_send()
         return carry
 
-    lax.fori_loop(1, n_ep, kv_done, 0)
+    lax.fori_loop(1, nz, kv_done, 0)
 
 
 def per_device(
@@ -333,27 +383,8 @@
     need = max(2, 3 * top * tokens // (2 * n_ep))
     cap = -(-need // 16) * 16
     slots = n_ep * cap
-    x = moe_in.astype(jnp.float32)
-    scale = lax.rsqrt(jnp.mean(x * x, axis=-1, keepdims=True) + EPSILON)
-    first = lax.axis_index("tp") * dq
-    x = lax.dynamic_slice_in_dim(moe_in, first, dq, 1).astype(jnp.float32)
-    normed = (x * scale * lax.dynamic_slice_in_dim(pre_gain, first, dq, 0)).astype(bf16)
-    slot = jnp.arange(slots, dtype=jnp.int32)[None, :]
-    route_weight = jax.nn.softmax(route_logits, axis=-1)
-    named = jnp.zeros((tokens, slots), jnp.bool_)
-    share = jnp.zeros((tokens, slots), jnp.float32)
-    for j in range(top):
-        hit = routes[:, j : j + 1] == slot // cap
-        named = named | hit
-        share = share + jnp.where(hit, route_weight[:, j : j + 1], 0.0)
-    earlier = jnp.tril(jnp.ones((tokens, tokens), bf16), -1)
-    rank = jnp.dot(earlier, named.astype(bf16), preferred_element_type=jnp.float32)
-    placed = named & (rank == (slot % cap).astype(jnp.float32))
-    mixw = jnp.where(placed, share, 0.0)
-    outgo = lax.dot_general(
-        placed.astype(bf16), normed, (((0,), (0,)), ((), ())),
-        preferred_element_type=jnp.float32,
-    ).astype(bf16)
+    slot = jnp.arange(slots, dtype=jnp.int32)
+    ids = jnp.stack([slot // cap, slot % cap])
 
     piece = rows // n_tp
     ff = w_gate.shape[2]
@@ -366,9 +397,11 @@
             jax.ShapeDtypeStruct((piece, width), bf16),
             jax.ShapeDtypeStruct((tokens, dq), bf16),
         ),
-        in_specs=[vmem] * 6 + [hbm] * 3,
+        in_specs=[vmem] * 9 + [hbm] * 3,
         out_specs=(vmem, vmem),
         scratch_shapes=[
+            pltpu.VMEM((slots, dq), bf16),
+            pltpu.VMEM((tokens, slots), jnp.float32),
             pltpu.VMEM((width, ff), bf16),
             pltpu.VMEM((width, ff), bf16),
             pltpu.VMEM((ff, width), bf16),
@@ -397,7 +430,7 @@
         compiler_params=pltpu.CompilerParams(
             collective_id=0, has_side_effects=True, vmem_limit_bytes=60 * 1024 * 1024
         ),
-    )(queries, paired, outgo, mixw, w_out, post_gain[None, :], w_gate[0], w_up[0], w_down[0])
+    )(queries, paired, moe_in, routes, route_logits, pre_gain[None, :], ids, w_out, post_gain[None, :], w_gate[0], w_up[0], w_down[0])
 
 
 def solution(mesh):

time: 103 us -> 91.9 us (0.89)
  Pallas kernels: 82.5 us -> 75 us
  matrix products: 2.96 us -> 0 us
  other arithmetic: 9.62 us -> 6.86 us
  local copies, waits for them, and re-layouts: 6.42 us -> 8.64 us
    pallas_call x1, Pallas kernels: 82.5 us -> 75 us  [per_device(): pl.pallas_call(functools.partial(kernel, (n_ep, n_tp, heads, cap)), out_s...]
    unnamed x9, local copies, waits for them, and re-layouts: 3.61 us -> 7.36 us
    dot_general x2 -> x0, matrix products: 2.96 us -> none  [the longest x1 2.01 us: per_device(): lax.dot_general(placed.astype(bf16), normed, (((0,), (0,)), ((), ())), pr...]
    reduce_sum x2 -> x0, other arithmetic: 1.93 us -> none  [the longest x1 1.23 us: per_device(): scale = lax.rsqrt(jnp.mean(x * x, axis=-1, keepdims=True) + EPSILON)]
    another operation x2 -> x3, other arithmetic: 2.48 us -> 3.06 us
where the time goes in v2:
time: 91.9 us; the launch traced here: 91.3 us
  Pallas kernels  75 us (82%)
  local copies, waits for them, and re-layouts  8.64 us (9%)
  other arithmetic  6.86 us (7%)
    pallas_call x1, Pallas kernels, per_device(): pl.pallas_call(functools.partial(kernel, (n_ep, n_tp, heads, cap)), out_s...  75 us
    unnamed x9, local copies, waits for them, and re-layouts  7.36 us
    another operation x2, other arithmetic  2.48 us

profile of v2, /device:TPU:9, one launch (start us, length us, event | category | flops | bytes accessed | tf_op | source)
XLA Modules:
  0.0 91.3 jit_solution(15770037328225396754)
XLA Ops:
  0.6 0.0 copy-start
  0.6 0.0 copy-start.1
  0.7 1.2 %fusion.10 = f32[512]{0:T(512)S(1)} fusion(bf16[512,256]{1,0:T(8,128)(2,1)} %param.15, s32[]{:T(128)S(6)} %select_n.59), kind=kLoop, calls=%fused_computation.18 | loop fusion | flops 97792 | bytes 67588 | tf_op jit(solution)/shard_map/reduce_sum | solution.py:17
  1.9 0.6 pad_add_fusion.ids_ref
  2.5 1.4 %copy.27.route_ref = s32[128,2]{1,0:T(8,128)} copy(s32[128,2]{0,1:T(2,128)} %param.22) | data formatting | bytes 2048 | tf_op args[8]
  3.9 1.4 %copy.28.logit_ref = f32[128,2]{1,0:T(8,128)} copy(f32[128,2]{0,1:T(2,128)} %param.23) | data formatting | bytes 2048 | tf_op args[9]
  5.3 0.0 copy-done
  5.3 0.1 constant_dynamic-slice_fusion
  5.4 0.3 multiply_cosine_fusion.3
  5.7 1.1 %fusion.12 = f32[512,1,64]{2,0,1:T(8,128)S(1)} fusion(f32[64]{0:T(128)} %param.18, f32[512]{0:T(512)S(1)} %add_rsqrt_fusion.1, bf16[512,256]{1,0:T(8,128)(2,1)} %param.15, s32[]{:T(128)S(6)} %select_n.59), kind=kLoop, calls=%fused_computation.20 | loop fusion | flops 98304 | bytes 198916 | tf_op jit(solution)/shard_map/mul | solution.py:17
  6.8 2.4 %fusion.18 = (bf16[512,1,16]{2,0,1:T(8,128)(2,1)S(1)}, bf16[512,1,16]{2,0,1:T(8,128)(2,1)S(1)}, bf16[512,1,16]{2,0,1:T(8,128)(2,1)S(1)}, bf16[512,1,16]{2,0,1:T(8,128)(2,1)S(1)}) fusion(f32[512,1,64]{2,0,1:T(8,128)S(1)} %fusion.12, f32[512]{0:T(512)S(1)} %get-tuple-element.20, f32[16]{0:T(128)S(1)} %multiply_power_fusion, f32[512]{0:T(512)S(1)} %get-tuple-element.21), kind=kLoop, calls=%fused_computation.26 | loop fusion | flops 147456 | bytes 200768 | tf_op jit(solution)/shard_map/convert.1
  9.2 0.2 maximum_bitcast_fusion
  9.4 0.8 pad_maximum_fusion.pair_ref
  10.2 1.1 %copy.23 = bf16[512,256]{0,1:T(8,128)(2,1)S(1)} copy(bf16[512,256]{1,0:T(8,128)(2,1)} %param.14) | data formatting | bytes 524288 | tf_op args[0]
  11.3 0.1 fusion
  11.4 0.0 copy-done.1
  11.4 0.1 fusion.1
  11.5 0.1 subtract_convert_fusion.1
  11.6 0.3 copy.24
  11.9 0.9 concatenate.15.q_ref
  12.8 75.0 %shard_map.149 = (bf16[128,2048]{1,0:T(8,128)(2,1)}, bf16[128,512]{1,0:T(8,128)(2,1)}) custom-call(bf16[2048,128]{1,0:T(8,128)(2,1)} %concatenate.15.q_ref, bf16[512,128]{1,0:T(8,128)(2,1)} %pad_maximum_fusion.pair_ref, bf16[128,2048]{1,0:T(8,128)(2,1)} %x_ref.1, s32[128,2]{1,0:T(8,128)} %copy.27.route_ref, f32[128,2]{1,0:T(8,128)} %copy.28.logit_ref, ...), custom_call_target="tpu_custom_call" | custom-call | tf_op jit(solution)/shard_map/pallas_call | solution.py:394
  87.8 1.9 %copy.31 = bf16[128,2048]{1,0:T(8,128)(2,1)} copy(bf16[128,2048]{1,0:T(8,128)(2,1)} %get-tuple-element.26) | data formatting | bytes 1048576
  89.7 1.6 %copy.32 = bf16[128,512]{1,0:T(8,128)(2,1)} copy(bf16[128,512]{1,0:T(8,128)(2,1)} %get-tuple-element.27) | data formatting | bytes 262144
  (6 shorter events, 0.1 us)
Async XLA Ops:
  0.6 4.7 %copy-start = (bf16[512,256]{1,0:T(8,128)(2,1)S(1)}, bf16[512,256]{1,0:T(8,128)(2,1)}, u32[]{:S(2)}) copy-start(bf16[512,256]{1,0:T(8,128)(2,1)} %param.16) | copy-start | bytes 786436
  0.6 10.7 %copy-start.1 = (f32[64]{0:T(128)S(1)}, f32[64]{0:T(128)}, u32[]{:S(2)}) copy-start(f32[64]{0:T(128)} %param.17) | copy-start | bytes 772
